TPU v7x, 32 devices: a whole 2x2x4 slice. The times are simulated.
32 devices in a mesh: sp: 8 (over z, y), tp: 4 (over x, core).
Axes of the slice: x: 2, y: 2, z: 4, core: 2. Of those that a mesh axis runs over, the one named last changes fastest.
Arguments:
- residual: bfloat16 [1024, 2048], P(('sp', 'tp')), may hold values from -6 to 6
- query_content: bfloat16 [1024, 1024], P('sp', 'tp'), may hold values from -400 to 400
- query_rotary: bfloat16 [1024, 384], P('sp', 'tp'), may hold values from -16 to 16
- key_latent: bfloat16 [1024, 512], P('sp'), may hold values from -6 to 6
- rotary_key: bfloat16 [1024, 32], P('sp'), may hold values from -6 to 6
- latent_gain: float32 [512], replicated, may hold values from 0.1 to 1.9
- key_weight: bfloat16 [512, 1024], P(None, 'tp'), may hold values from -0.25 to 0.25
- value_weight: bfloat16 [512, 1024], P(None, 'tp'), may hold values from -0.25 to 0.25
- output_gain: float32 [1024], P('tp'), may hold values from 0.1 to 1.9
- output_weight: bfloat16 [1024, 2048], P('tp'), may hold values from -0.1875 to 0.1875
- mixer_gain: float32 [2048], replicated, may hold values from 0.1 to 1.9
- gate_weight: bfloat16 [2048, 5632], P('sp', 'tp'), may hold values from -0.125 to 0.125
- up_weight: bfloat16 [2048, 5632], P('sp', 'tp'), may hold values from -0.125 to 0.125
- down_weight: bfloat16 [5632, 2048], P('tp', 'sp'), may hold values from -0.078125 to 0.078125
Outputs:
- layer_out: bfloat16 [1024, 2048], P(('sp', 'tp'))
All inputs are finite; a program needn't handle non-finite values.
Results may differ from a plain program's by a relative error of at most 0.015.
Values may be sent and summed in bfloat16 or wider, within the bound.
A program may use at most 128 MiB of HBM per device.

v0:
```python
import functools

import jax
import jax.numpy as jnp
import numpy as np
from jax import lax
from jax.experimental import pallas as pl
from jax.experimental.pallas import tpu as pltpu
from jax.sharding import PartitionSpec as P

NARROW_HEADS = 8
WIDE_HEADS = 4
NARROW_DIM = 64
WIDE_DIM = 128
ROT_DIM = 32


epsilon = 1e-06
rope_base = 500000.0


def normalize(values):
    values = values.astype(jnp.float32)
    return values * lax.rsqrt(jnp.mean(values * values, axis=-1, keepdims=True) + epsilon)


def rotate(values, positions):
    half_width = values.shape[-1] // 2
    inverse = 1.0 / jnp.power(
        rope_base, jnp.arange(0, 2 * half_width, 2, dtype=jnp.float32) / (2 * half_width)
    )
    angles = positions.astype(jnp.float32)[:, None] * inverse[None, :]
    table_shape = (angles.shape[0],) + (1,) * (values.ndim - 2) + (half_width,)
    cosine_table = jnp.cos(angles).reshape(table_shape)
    sine_table = jnp.sin(angles).reshape(table_shape)
    first_half = values[..., :half_width]
    second_half = values[..., half_width:]
    return jnp.concatenate(
        [
            first_half * cosine_table - second_half * sine_table,
            second_half * cosine_table + first_half * sine_table,
        ],
        axis=-1,
    )


def group_update(carried, query_part, rotary_part, key_part, rotary_keys, value_part, factor):
    running_max, totals, accumulated = carried
    scores = (
        jnp.einsum("qhd,khd->hqk", query_part, key_part, preferred_element_type=jnp.float32)
        + jnp.einsum("qhd,kd->hqk", rotary_part, rotary_keys, preferred_element_type=jnp.float32)
    ) * factor
    new_max = jnp.max(scores, axis=-1)
    shrink = jnp.exp(running_max - new_max)
    powers = jnp.exp(scores - new_max[..., None])
    totals = totals * shrink + jnp.sum(powers, axis=-1)
    added = jnp.einsum(
        "hqk,khd->qhd", powers.astype(jnp.bfloat16), value_part, preferred_element_type=jnp.float32
    )
    accumulated = accumulated * jnp.transpose(shrink)[:, :, None] + added
    return (new_max, totals, accumulated)


def on_device(
    residual,
    query_content,
    query_rotary,
    key_latent,
    rotary_key,
    latent_gain,
    key_weight,
    value_weight,
    output_gain,
    output_weight,
    mixer_gain,
    gate_weight,
    up_weight,
    down_weight,
):
    tp_count = lax.axis_size("tp")
    narrow_dev = NARROW_HEADS // tp_count
    wide_dev = WIDE_HEADS // tp_count
    row_count = key_latent.shape[0]
    positions = lax.axis_index("sp") * row_count + lax.iota(jnp.int32, row_count)
    latent = (normalize(key_latent) * latent_gain).astype(jnp.bfloat16)
    key_rows = jnp.dot(latent, key_weight, preferred_element_type=jnp.float32).astype(jnp.bfloat16)
    value_rows = jnp.dot(latent, value_weight, preferred_element_type=jnp.float32).astype(
        jnp.bfloat16
    )
    rot_keys = rotate(rotary_key.astype(jnp.float32), positions).astype(jnp.bfloat16)
    head_count = narrow_dev + wide_dev
    rot_queries = rotate(
        query_rotary.astype(jnp.float32).reshape(row_count, head_count, ROT_DIM), positions
    ).astype(jnp.bfloat16)
    narrow_cols = narrow_dev * NARROW_DIM
    query_narrow = query_content[:, :narrow_cols].reshape(row_count, narrow_dev, NARROW_DIM)
    query_wide = query_content[:, narrow_cols:].reshape(row_count, wide_dev, WIDE_DIM)
    rotary_narrow = rot_queries[:, :narrow_dev]
    rotary_wide = rot_queries[:, narrow_dev:]
    narrow_factor = (NARROW_DIM + ROT_DIM) ** (-0.5)
    wide_factor = (WIDE_DIM + ROT_DIM) ** (-0.5)

    def start_state(count, width):
        return (
            jnp.full((count, row_count), -jnp.inf, jnp.float32),
            jnp.zeros((count, row_count), jnp.float32),
            jnp.zeros((row_count, count, width), jnp.float32),
        )

    carried = (start_state(narrow_dev, NARROW_DIM), start_state(wide_dev, WIDE_DIM))
    piece_keys = lax.all_gather(key_rows, "sp", axis=0, tiled=True)
    piece_rotary = lax.all_gather(rot_keys, "sp", axis=0, tiled=True)
    piece_values = lax.all_gather(value_rows, "sp", axis=0, tiled=True)
    length = piece_keys.shape[0]
    narrow_keys = piece_keys[:, :narrow_cols].reshape(length, narrow_dev, NARROW_DIM)
    wide_keys = piece_keys[:, narrow_cols:].reshape(length, wide_dev, WIDE_DIM)
    narrow_values = piece_values[:, :narrow_cols].reshape(length, narrow_dev, NARROW_DIM)
    wide_values = piece_values[:, narrow_cols:].reshape(length, wide_dev, WIDE_DIM)
    narrow_state = group_update(
        carried[0],
        query_narrow,
        rotary_narrow,
        narrow_keys,
        piece_rotary,
        narrow_values,
        narrow_factor,
    )
    wide_state = group_update(
        carried[1], query_wide, rotary_wide, wide_keys, piece_rotary, wide_values, wide_factor
    )
    narrow_state, wide_state = (narrow_state, wide_state)

    def finish(carried):
        return normalize(carried[2] / jnp.transpose(carried[1])[:, :, None]).reshape(row_count, -1)

    mixed = (
        jnp.concatenate([finish(narrow_state), finish(wide_state)], axis=1) * output_gain
    ).astype(jnp.bfloat16)
    whole_output = lax.all_gather(output_weight, "tp", axis=0, tiled=True)
    regrouped = lax.all_to_all(mixed, "tp", split_axis=0, concat_axis=1, tiled=True)
    projected = jnp.dot(regrouped, whole_output, preferred_element_type=jnp.float32)
    middle = (residual.astype(jnp.float32) + projected).astype(jnp.bfloat16)
    normed = (normalize(middle) * mixer_gain).astype(jnp.bfloat16)
    block_normed = lax.all_gather(normed, "tp", axis=0, tiled=True)
    gate_sums = jnp.dot(
        block_normed,
        lax.all_gather(gate_weight, "sp", axis=0, tiled=True),
        preferred_element_type=jnp.float32,
    )
    up_sums = jnp.dot(
        block_normed,
        lax.all_gather(up_weight, "sp", axis=0, tiled=True),
        preferred_element_type=jnp.float32,
    )
    down_whole = lax.all_gather(down_weight, "sp", axis=1, tiled=True)
    hidden = (jax.nn.silu(gate_sums) * up_sums).astype(jnp.bfloat16)
    channel_out = lax.psum_scatter(
        jnp.dot(hidden, down_whole, preferred_element_type=jnp.float32).astype(jnp.bfloat16),
        "tp",
        scatter_dimension=0,
        tiled=True,
    ).astype(jnp.float32)
    return (middle.astype(jnp.float32) + channel_out).astype(jnp.bfloat16)


MESH = pl.DeviceIdType.MESH
LANES = 128
PAIR = 2


def kernel(
    n_sp,
    query_ref,
    latent_ref,
    latent_gain_ref,
    key_weight_ref,
    value_weight_ref,
    output_gain_ref,
    mixer_gain_ref,
    cos_ref,
    sin_ref,
    swap_ref,
    residual_ref,
    output_weight_ref,
    gate_ref,
    up_ref,
    down_ref,
    turn_hbm,
    rotary_ref,
    out_ref,
    turn_ref,
    lat_all,
    rot_all,
    keys,
    values,
    res_all,
    out_all,
    mix_all,
    middle,
    normed,
    gate_all,
    up_all,
    down_all,
    hidden,
    part,
    from_core,
    to_x,
    from_x,
    to_z,
    from_z,
    summed_up,
    send_sems,
    recv_sems,
    local_sems,
):
    n_z = n_sp // PAIR
    s = lax.axis_index("sp")
    t = lax.axis_index("tp")
    z, y = s // PAIR, lax.rem(s, PAIR)
    x, c = t // PAIR, lax.rem(t, PAIR)
    rows, depth = latent_ref.shape
    half = rows // PAIR
    sibling = (s, x * PAIR + 1 - c)
    across = (s, (1 - x) * PAIR + c)
    beside = (z * PAIR + 1 - y, t)
    f32 = jnp.float32

    def z_id(step):
        return (lax.rem(z + step, n_z) * PAIR + y, t)

    barrier = pltpu.get_barrier_semaphore()
    greeted = [(lax.rem(s + k, n_sp), t) for k in range(1, n_sp)] + [sibling, across]
    for device in greeted:
        pl.semaphore_signal(barrier, inc=1, device_id=device, device_id_type=MESH)

    used = [0]
    locals_used = [0]
    sent = []

    def local(src, dst):
        copy = pltpu.make_async_copy(src, dst, local_sems.at[locals_used[0]])
        locals_used[0] += 1
        copy.start()
        return copy

    def send(src, dst, device):
        copy = pltpu.make_async_remote_copy(
            src_ref=src,
            dst_ref=dst,
            send_sem=send_sems.at[used[0]],
            recv_sem=recv_sems.at[used[0]],
            device_id=device,
            device_id_type=MESH,
        )
        used[0] += 1
        copy.start()
        sent.append(copy)
        return copy

    width = gate_all.shape[1]
    total_width = gate_ref.shape[1]
    slab = gate_ref.shape[0]

    def first(piece):
        return pl.multiple_of(jnp.minimum(piece * width, total_width - width), LANES)

    def span(owner):
        return pl.ds(pl.multiple_of(owner * slab, slab), slab)

    mine = span(s)
    my_piece = pl.ds(first(z), width)
    half_rows = pl.ds(pl.multiple_of(c * half, half), half)
    here = pl.ds(pl.multiple_of(s * rows, rows), rows)
    locals_first = [
        local(latent_ref, lat_all.at[here]),
        local(rotary_ref, rot_all.at[here]),
        local(turn_hbm, turn_ref),
    ]
    down_cols = pl.ds(pl.multiple_of(y * slab, slab), slab)
    locals_rest = [
        local(residual_ref, res_all.at[x, c, z]),
        local(output_weight_ref, out_all.at[x, c]),
        local(gate_ref.at[:, my_piece], gate_all.at[mine]),
        local(up_ref.at[:, my_piece], up_all.at[mine]),
        local(down_ref.at[my_piece], down_all.at[0, :, down_cols]),
    ]
    pl.semaphore_wait(barrier, len(greeted))

    def token_half(owner):
        return pl.ds(pl.multiple_of(owner * rows + c * half, half), half)

    def send_latent(device):
        return (
            send(latent_ref.at[half_rows], lat_all.at[token_half(s)], device),
            send(rotary_ref.at[half_rows], rot_all.at[token_half(s)], device),
        )

    def pass_latent(owner, device):
        place = token_half(owner)
        return (
            send(lat_all.at[place], lat_all.at[place], device),
            send(rot_all.at[place], rot_all.at[place], device),
        )

    def piece_of(step):
        return pl.ds(first(lax.rem(z + step, n_z)), width)

    latent_z = [send_latent(z_id(k)) for k in range(1, n_z)]
    latent_y = [send_latent(beside)]
    weight_x = send(output_weight_ref, out_all.at[x, c], across)
    gate_z = [
        send(gate_ref.at[:, piece_of(k)], gate_all.at[mine], z_id(k)) for k in range(1, n_z)
    ]
    z_far = lax.rem(z + PAIR, n_z)
    z_near = z + 1 - 2 * lax.rem(z, PAIR)
    near = (z_near * PAIR + y, t)
    residual_a = send(residual_ref, res_all.at[x, c, z], z_id(PAIR))

    latent_core = []
    for step in range(1, n_z):
        for copy in latent_z[step - 1]:
            copy.wait_recv()
        owner = lax.rem(z + n_z - step, n_z) * PAIR + y
        latent_y.append(pass_latent(owner, beside))
        latent_core.extend(pass_latent(owner, sibling))
    weight_y = [
        send(gate_ref.at[:, my_piece], gate_all.at[mine], beside),
        send(up_ref.at[:, my_piece], up_all.at[mine], beside),
        send(down_ref.at[my_piece], down_all.at[0, :, down_cols], beside),
    ]
    for step in range(n_z):
        for copy in latent_y[step]:
            copy.wait_recv()
        owner = lax.rem(z + n_z - step, n_z) * PAIR + 1 - y
        latent_core.extend(pass_latent(owner, sibling))
    weight_core = send(output_weight_ref, out_all.at[x, c], sibling)
    for copy in locals_first:
        copy.wait()
    for copy in latent_core:
        copy.wait_recv()

    gain = latent_gain_ref[...]

    def project(block, _):
        place = pl.ds(pl.multiple_of(block * rows, rows), rows)
        raw = lat_all[place, :].astype(f32)
        scale = lax.rsqrt(jnp.mean(raw * raw, axis=-1, keepdims=True) + epsilon)
        latent = (raw * scale * gain).astype(jnp.bfloat16)
        keys[place, :] = jnp.dot(latent, key_weight_ref[...], preferred_element_type=f32).astype(
            jnp.bfloat16
        )
        values[place, :] = jnp.dot(
            latent, value_weight_ref[...], preferred_element_type=f32
        ).astype(jnp.bfloat16)
        return 0

    lax.fori_loop(0, n_sp, project, 0)
    rot_width = rot_all.shape[1]
    rot_raw = rot_all[...]
    swap = swap_ref[...]
    rot_swapped = jnp.dot(rot_raw, swap[:rot_width, :rot_width], preferred_element_type=f32)
    rot_keys = (
        rot_raw.astype(f32) * cos_ref[:, :rot_width] + rot_swapped * sin_ref[:, :rot_width]
    ).astype(jnp.bfloat16)
    turn_raw = turn_ref[...]
    turn_swapped = jnp.dot(turn_raw, swap, preferred_element_type=f32)
    turned = (turn_raw.astype(f32) * cos_ref[here, :] + turn_swapped * sin_ref[here, :]).astype(
        jnp.bfloat16
    )

    content = query_ref.shape[1]
    head_count = turn_ref.shape[1] // rot_width
    wide_dev = (content - head_count * NARROW_DIM) // (WIDE_DIM - NARROW_DIM)
    sizes = [NARROW_DIM] * (head_count - wide_dev) + [WIDE_DIM] * wide_dev
    contract = (((1,), (1,)), ((), ()))
    heads = []
    start = 0
    for index, size in enumerate(sizes):
        cols = slice(start, start + size)
        scores = lax.dot_general(
            query_ref[:, cols], keys[:, cols], contract, preferred_element_type=f32
        )
        scores = scores + lax.dot_general(
            turned[:, index * rot_width : (index + 1) * rot_width],
            rot_keys,
            contract,
            preferred_element_type=f32,
        )
        scores = scores * (size + ROT_DIM) ** (-0.5)
        powers = jnp.exp(scores - jnp.max(scores, axis=-1, keepdims=True))
        totals = jnp.sum(powers, axis=-1, keepdims=True)
        summed = jnp.dot(
            powers.astype(jnp.bfloat16), values[:, cols], preferred_element_type=f32
        )
        attended = summed / totals
        scale = lax.rsqrt(jnp.mean(attended * attended, axis=-1, keepdims=True) + epsilon)
        heads.append(attended * scale)
        start += size
    mixed = (jnp.concatenate(heads, axis=1) * output_gain_ref[...]).astype(jnp.bfloat16)
    mix_all[x, c, z] = mixed

    mix_z = [send(mix_all.at[x, c, z], mix_all.at[x, c, z], z_id(k)) for k in range(1, n_z)]

    def relay(copies, buffer, step):
        copies[step - 1].wait_recv()
        block = buffer.at[span(lax.rem(z + n_z - step, n_z) * PAIR + y)]
        return send(block, block, beside)

    gate_y = [relay(gate_z, gate_all, k) for k in range(1, n_z)]
    residual_a.wait_recv()
    locals_rest[0].wait()
    residual_b = [
        send(res_all.at[x, c, block], res_all.at[x, c, block], near) for block in (z, z_far)
    ]
    up_z = [send(up_ref.at[:, piece_of(k)], up_all.at[mine], z_id(k)) for k in range(1, n_z)]
    down_z = [
        send(down_ref.at[piece_of(k)], down_all.at[k, :, down_cols], z_id(k))
        for k in range(1, n_z)
    ]

    for copy in locals_rest[1:]:
        copy.wait()
    weight_x.wait_recv()
    weight_far = send(out_all.at[1 - x, c], out_all.at[1 - x, c], sibling)
    for copy in mix_z:
        copy.wait_recv()
    mix_x = send(mix_all.at[x, c], mix_all.at[x, c], across)
    mix_core = send(mix_all.at[x, c], mix_all.at[x, c], sibling)
    for copy in residual_b:
        copy.wait_recv()
    residual_x = send(res_all.at[x, c], res_all.at[x, c], across)
    residual_core = send(res_all.at[x, c], res_all.at[x, c], sibling)
    mix_x.wait_recv()
    mix_far = send(mix_all.at[1 - x, c], mix_all.at[1 - x, c], sibling)
    up_y = [relay(up_z, up_all, 1)]
    residual_x.wait_recv()
    residual_far = send(res_all.at[1 - x, c], res_all.at[1 - x, c], sibling)
    up_y += [relay(up_z, up_all, k) for k in range(2, n_z)]
    for copy in (weight_core, weight_far, mix_core, mix_far, residual_core, residual_far):
        copy.wait_recv()

    mixer_gain = mixer_gain_ref[...]
    d_model = middle.shape[1]

    def finish_rows(block, _):
        place = pl.ds(pl.multiple_of(block * rows, rows), rows)
        total = res_all[:, :, block].reshape(rows, d_model).astype(f32)
        projected = jnp.zeros((rows, d_model), f32)
        for far in range(PAIR):
            for core in range(PAIR):
                projected = projected + jnp.dot(
                    mix_all[far, core, block], out_all[far, core], preferred_element_type=f32
                )
        mid = (total + projected).astype(jnp.bfloat16)
        middle[place, :] = mid
        wide = mid.astype(f32)
        scale = lax.rsqrt(jnp.mean(wide * wide, axis=-1, keepdims=True) + epsilon)
        normed[place, :] = (wide * scale * mixer_gain).astype(jnp.bfloat16)
        return 0

    lax.fori_loop(0, n_z, finish_rows, 0)

    def relay_down(step):
        down_z[step - 1].wait_recv()
        block = down_all.at[step, :, down_cols]
        return send(block, block, beside)

    down_y = [weight_y[2], relay_down(1)]
    for copy in gate_y + up_y + weight_y[:2]:
        copy.wait_recv()

    lane = lax.broadcasted_iota(jnp.int32, (rows, width), 1)
    fresh = lane + first(z) >= z * width

    def units(block, _):
        place = pl.ds(pl.multiple_of(block * rows, rows), rows)
        left = normed[place, :]
        gates = jnp.dot(left, gate_all[...], preferred_element_type=f32)
        ups = jnp.dot(left, up_all[...], preferred_element_type=f32)
        value = gates / (1.0 + jnp.exp(-gates)) * ups
        hidden[place, :] = jnp.where(fresh, value, 0.0).astype(jnp.bfloat16)
        return 0

    lax.fori_loop(0, n_z, units, 0)

    core_copies, x_copies, z_copies = [], [], []
    for step in range(n_z + 2):
        n = step - 2
        if 0 <= n < n_z:
            x_copies[n].wait_recv()
            to_z[n] = (to_x[n, :, x].astype(f32) + from_x[n].astype(f32)).astype(jnp.bfloat16)
            z_copies.append(
                [
                    send(to_z.at[n, lax.rem(z + k, n_z)], from_z.at[n, k - 1], z_id(k))
                    for k in range(1, n_z)
                ]
            )
        n = step - 1
        if 0 <= n < n_z:
            core_copies[n].wait_recv()
            to_x[n] = (part[n, :, :, c].astype(f32) + from_core[n].astype(f32)).astype(
                jnp.bfloat16
            )
            x_copies.append(send(to_x.at[n, :, 1 - x], from_x.at[n], across))
        n = step
        if n < n_z:
            if 2 <= n + 1 < n_z:
                down_y.append(relay_down(n + 1))
            down_y[n].wait_recv()
            product = jnp.dot(hidden[...], down_all[n], preferred_element_type=f32)
            part[n] = product.astype(jnp.bfloat16).reshape(part.shape[1:])
            core_copies.append(send(part.at[n, :, :, 1 - c], from_core.at[n], sibling))
    strip = out_ref.shape[0]
    chunk = part.shape[-1]
    own = pl.ds(pl.multiple_of(z * rows + t * strip, strip), strip)

    def cols_of(back):
        return pl.ds(pl.multiple_of(lax.rem(z + 2 * n_z - back, n_z) * chunk, chunk), chunk)

    for n in range(n_z):
        cols = cols_of(n)
        summed_up[:, cols] = middle[own, cols].astype(f32) + to_z[n, z].astype(f32)
    for n in range(n_z):
        for k in range(1, n_z):
            z_copies[n][k - 1].wait_recv()
            cols = cols_of(n + k)
            summed_up[:, cols] = summed_up[:, cols] + from_z[n, k - 1].astype(f32)
    out_ref[...] = summed_up[...].astype(jnp.bfloat16)
    for copy in sent:
        copy.wait_send()


def fused(
    n_sp,
    residual,
    query_content,
    query_rotary,
    key_latent,
    rotary_key,
    latent_gain,
    key_weight,
    value_weight,
    output_gain,
    output_weight,
    mixer_gain,
    gate_weight,
    up_weight,
    down_weight,
):
    n_z = n_sp // PAIR
    rows, latent_width = key_latent.shape
    strip, d_model = residual.shape
    tokens = rows * n_sp
    content = query_content.shape[1]
    turn_width = query_rotary.shape[1]
    half_width = ROT_DIM // 2
    inverse = np.float32(1.0) / np.power(
        np.float32(rope_base), np.arange(0, ROT_DIM, 2, dtype=np.float32) / np.float32(ROT_DIM)
    )
    angles = np.arange(tokens, dtype=np.float32)[:, None] * inverse[None, :].astype(np.float32)
    head_count = turn_width // ROT_DIM
    cosine = np.cos(angles).astype(np.float32)
    sine = np.sin(angles).astype(np.float32)
    cos_table = np.tile(np.concatenate([cosine, cosine], axis=1), (1, head_count))
    sin_table = np.tile(np.concatenate([-sine, sine], axis=1), (1, head_count))
    lane = np.arange(turn_width)
    other = lane // ROT_DIM * ROT_DIM + (lane + half_width) % ROT_DIM
    swap = np.zeros((turn_width, turn_width), np.float32)
    swap[other, lane] = 1.0
    tiles = gate_weight.shape[1] // LANES
    width = -(-tiles // n_z) * LANES
    slab = rows * n_z
    chunk = d_model // n_z
    bf16 = jnp.bfloat16
    n_copies = 4 * n_sp + 8 * n_z + 20 + n_z * (n_z + 1)
    vmem = pl.BlockSpec(memory_space=pltpu.VMEM)
    anywhere = pl.BlockSpec(memory_space=pl.ANY)
    return pl.pallas_call(
        functools.partial(kernel, n_sp),
        out_shape=jax.ShapeDtypeStruct((strip, d_model), bf16),
        in_specs=[vmem] * 10 + [anywhere] * 7,
        out_specs=vmem,
        scratch_shapes=[
            pltpu.VMEM((rows, turn_width), bf16),
            pltpu.VMEM((tokens, latent_width), bf16),
            pltpu.VMEM((tokens, ROT_DIM), bf16),
            pltpu.VMEM((tokens, content), bf16),
            pltpu.VMEM((tokens, content), bf16),
            pltpu.VMEM((PAIR, PAIR, n_z, strip, d_model), bf16),
            pltpu.VMEM((PAIR, PAIR, content, d_model), bf16),
            pltpu.VMEM((PAIR, PAIR, n_z, rows, content), bf16),
            pltpu.VMEM((slab, d_model), bf16),
            pltpu.VMEM((slab, d_model), bf16),
            pltpu.VMEM((d_model, width), bf16),
            pltpu.VMEM((d_model, width), bf16),
            pltpu.VMEM((n_z, width, chunk), bf16),
            pltpu.VMEM((slab, width), bf16),
            pltpu.VMEM((n_z, n_z, PAIR, PAIR, strip, chunk), bf16),
            pltpu.VMEM((n_z, n_z, PAIR, strip, chunk), bf16),
            pltpu.VMEM((n_z, n_z, PAIR, strip, chunk), bf16),
            pltpu.VMEM((n_z, n_z, strip, chunk), bf16),
            pltpu.VMEM((n_z, n_z, strip, chunk), bf16),
            pltpu.VMEM((n_z, n_z - 1, strip, chunk), bf16),
            pltpu.VMEM((strip, d_model), jnp.float32),
            pltpu.SemaphoreType.DMA((n_copies,)),
            pltpu.SemaphoreType.DMA((n_copies,)),
            pltpu.SemaphoreType.DMA((8,)),
        ],
        compiler_params=pltpu.CompilerParams(
            collective_id=0, has_side_effects=True, vmem_limit_bytes=60 * 1024 * 1024
        ),
        name="layer",
    )(
        query_content,
        key_latent,
        latent_gain.reshape(1, -1),
        key_weight,
        value_weight,
        output_gain.reshape(1, -1),
        mixer_gain.reshape(1, -1),
        jnp.asarray(cos_table),
        jnp.asarray(sin_table),
        jnp.asarray(swap, dtype=bf16),
        residual,
        output_weight,
        gate_weight,
        up_weight,
        down_weight,
        query_rotary,
        rotary_key,
    )


def solution(mesh):
    n_sp, n_tp = mesh.shape["sp"], mesh.shape["tp"]

    def program(*arrays):
        residual, gate_weight = arrays[0], arrays[11]
        fits = (
            n_tp == PAIR * PAIR
            and n_sp == PAIR**3
            and gate_weight.shape[0] * n_sp == residual.shape[1]
            and gate_weight.shape[0] % LANES == 0
            and gate_weight.shape[1] % LANES == 0
        )
        if fits:
            return fused(n_sp, *arrays)
        return on_device(*arrays)

    placed = (
        P(("sp", "tp"), None),
        P("sp", "tp"),
        P("sp", "tp"),
        P("sp", None),
        P("sp", None),
        P(),
        P(None, "tp"),
        P(None, "tp"),
        P("tp"),
        P("tp", None),
        P(),
        P("sp", "tp"),
        P("sp", "tp"),
        P("tp", "sp"),
    )
    return jax.shard_map(
        program, mesh=mesh, in_specs=placed, out_specs=P(("sp", "tp"), None), check_vma=False
    )
```

profile of v0, /device:TPU:0, one launch (start us, length us, event | category | flops | bytes accessed | tf_op | source)
XLA Modules:
  0.0 111.8 jit_solution(3891759829944476987)
XLA Ops:
  0.0 0.0 copy-start
  0.0 1.5 %copy.18.turn_hbm = bf16[128,96]{1,0:T(8,128)(2,1)} copy(bf16[128,96]{0,1:T(8,128)(2,1)} %param.19) | data formatting | bytes 49152 | tf_op args[2]
  1.5 0.0 copy-done
  1.5 0.7 copy.19.rotary_ref
  2.2 108.0 %layer.1 = bf16[32,2048]{1,0:T(8,128)(2,1)} custom-call(bf16[128,256]{1,0:T(8,128)(2,1)} %query_ref.1, bf16[128,512]{1,0:T(8,128)(2,1)} %latent_ref.1, f32[1,512]{1,0:T(1,128)} %bitcast.4, bf16[512,256]{1,0:T(8,128)(2,1)} %key_weight_ref.1, bf16[512,256]{1,0:T(8,128)(2,1)} %value_weight_ref.1, f32[1,256]{1,0:T(1,128)} %bitcast.5, f32[1,2048]{1,0:T(1,128)} %bitcast.3, ...), custom_call_target="tpu_custom_call" | custom-call | tf_op jit(solution)/shard_map/layer/pallas_call | solution.py:578
  110.2 1.6 %copy.21 = bf16[32,2048]{1,0:T(8,128)(2,1)} copy(bf16[32,2048]{1,0:T(8,128)(2,1)} %layer.1) | data formatting | bytes 262144
Async XLA Ops:
  0.0 1.5 %copy-start = (bf16[128,32]{0,1:T(8,128)(2,1)S(1)}, bf16[128,32]{0,1:T(8,128)(2,1)}, u32[]{:S(2)}) copy-start(bf16[128,32]{0,1:T(8,128)(2,1)} %param.21) | copy-start | bytes 24580
where the time goes:
time: 112 us
  Pallas kernels  108 us (96%)
  local copies, waits for them, and re-layouts  3.75 us (3%)
    pallas_call x1, Pallas kernels, fused(): pl.pallas_call(functools.partial(kernel, n_sp), out_shape=jax.ShapeDtypeS...  108 us
    unnamed x5, local copies, waits for them, and re-layouts  3.75 us

commit v1 on v0

v1 whole, which is shorter than its diff:
```python
import functools

import jax
import jax.numpy as jnp
import numpy as np
from jax import lax
from jax.experimental import pallas as pl
from jax.experimental.pallas import tpu as pltpu
from jax.sharding import PartitionSpec as P

NARROW_HEADS = 8
WIDE_HEADS = 4
NARROW_DIM = 64
WIDE_DIM = 128
ROT_DIM = 32


epsilon = 1e-06
rope_base = 500000.0


def normalize(values):
    values = values.astype(jnp.float32)
    return values * lax.rsqrt(jnp.mean(values * values, axis=-1, keepdims=True) + epsilon)


def rotate(values, positions):
    half_width = values.shape[-1] // 2
    inverse = 1.0 / jnp.power(
        rope_base, jnp.arange(0, 2 * half_width, 2, dtype=jnp.float32) / (2 * half_width)
    )
    angles = positions.astype(jnp.float32)[:, None] * inverse[None, :]
    table_shape = (angles.shape[0],) + (1,) * (values.ndim - 2) + (half_width,)
    cosine_table = jnp.cos(angles).reshape(table_shape)
    sine_table = jnp.sin(angles).reshape(table_shape)
    first_half = values[..., :half_width]
    second_half = values[..., half_width:]
    return jnp.concatenate(
        [
            first_half * cosine_table - second_half * sine_table,
            second_half * cosine_table + first_half * sine_table,
        ],
        axis=-1,
    )


def group_update(carried, query_part, rotary_part, key_part, rotary_keys, value_part, factor):
    running_max, totals, accumulated = carried
    scores = (
        jnp.einsum("qhd,khd->hqk", query_part, key_part, preferred_element_type=jnp.float32)
        + jnp.einsum("qhd,kd->hqk", rotary_part, rotary_keys, preferred_element_type=jnp.float32)
    ) * factor
    new_max = jnp.max(scores, axis=-1)
    shrink = jnp.exp(running_max - new_max)
    powers = jnp.exp(scores - new_max[..., None])
    totals = totals * shrink + jnp.sum(powers, axis=-1)
    added = jnp.einsum(
        "hqk,khd->qhd", powers.astype(jnp.bfloat16), value_part, preferred_element_type=jnp.float32
    )
    accumulated = accumulated * jnp.transpose(shrink)[:, :, None] + added
    return (new_max, totals, accumulated)


def on_device(
    residual,
    query_content,
    query_rotary,
    key_latent,
    rotary_key,
    latent_gain,
    key_weight,
    value_weight,
    output_gain,
    output_weight,
    mixer_gain,
    gate_weight,
    up_weight,
    down_weight,
):
    tp_count = lax.axis_size("tp")
    narrow_dev = NARROW_HEADS // tp_count
    wide_dev = WIDE_HEADS // tp_count
    row_count = key_latent.shape[0]
    positions = lax.axis_index("sp") * row_count + lax.iota(jnp.int32, row_count)
    latent = (normalize(key_latent) * latent_gain).astype(jnp.bfloat16)
    key_rows = jnp.dot(latent, key_weight, preferred_element_type=jnp.float32).astype(jnp.bfloat16)
    value_rows = jnp.dot(latent, value_weight, preferred_element_type=jnp.float32).astype(
        jnp.bfloat16
    )
    rot_keys = rotate(rotary_key.astype(jnp.float32), positions).astype(jnp.bfloat16)
    head_count = narrow_dev + wide_dev
    rot_queries = rotate(
        query_rotary.astype(jnp.float32).reshape(row_count, head_count, ROT_DIM), positions
    ).astype(jnp.bfloat16)
    narrow_cols = narrow_dev * NARROW_DIM
    query_narrow = query_content[:, :narrow_cols].reshape(row_count, narrow_dev, NARROW_DIM)
    query_wide = query_content[:, narrow_cols:].reshape(row_count, wide_dev, WIDE_DIM)
    rotary_narrow = rot_queries[:, :narrow_dev]
    rotary_wide = rot_queries[:, narrow_dev:]
    narrow_factor = (NARROW_DIM + ROT_DIM) ** (-0.5)
    wide_factor = (WIDE_DIM + ROT_DIM) ** (-0.5)

    def start_state(count, width):
        return (
            jnp.full((count, row_count), -jnp.inf, jnp.float32),
            jnp.zeros((count, row_count), jnp.float32),
            jnp.zeros((row_count, count, width), jnp.float32),
        )

    carried = (start_state(narrow_dev, NARROW_DIM), start_state(wide_dev, WIDE_DIM))
    piece_keys = lax.all_gather(key_rows, "sp", axis=0, tiled=True)
    piece_rotary = lax.all_gather(rot_keys, "sp", axis=0, tiled=True)
    piece_values = lax.all_gather(value_rows, "sp", axis=0, tiled=True)
    length = piece_keys.shape[0]
    narrow_keys = piece_keys[:, :narrow_cols].reshape(length, narrow_dev, NARROW_DIM)
    wide_keys = piece_keys[:, narrow_cols:].reshape(length, wide_dev, WIDE_DIM)
    narrow_values = piece_values[:, :narrow_cols].reshape(length, narrow_dev, NARROW_DIM)
    wide_values = piece_values[:, narrow_cols:].reshape(length, wide_dev, WIDE_DIM)
    narrow_state = group_update(
        carried[0],
        query_narrow,
        rotary_narrow,
        narrow_keys,
        piece_rotary,
        narrow_values,
        narrow_factor,
    )
    wide_state = group_update(
        carried[1], query_wide, rotary_wide, wide_keys, piece_rotary, wide_values, wide_factor
    )
    narrow_state, wide_state = (narrow_state, wide_state)

    def finish(carried):
        return normalize(carried[2] / jnp.transpose(carried[1])[:, :, None]).reshape(row_count, -1)

    mixed = (
        jnp.concatenate([finish(narrow_state), finish(wide_state)], axis=1) * output_gain
    ).astype(jnp.bfloat16)
    whole_output = lax.all_gather(output_weight, "tp", axis=0, tiled=True)
    regrouped = lax.all_to_all(mixed, "tp", split_axis=0, concat_axis=1, tiled=True)
    projected = jnp.dot(regrouped, whole_output, preferred_element_type=jnp.float32)
    middle = (residual.astype(jnp.float32) + projected).astype(jnp.bfloat16)
    normed = (normalize(middle) * mixer_gain).astype(jnp.bfloat16)
    block_normed = lax.all_gather(normed, "tp", axis=0, tiled=True)
    gate_sums = jnp.dot(
        block_normed,
        lax.all_gather(gate_weight, "sp", axis=0, tiled=True),
        preferred_element_type=jnp.float32,
    )
    up_sums = jnp.dot(
        block_normed,
        lax.all_gather(up_weight, "sp", axis=0, tiled=True),
        preferred_element_type=jnp.float32,
    )
    down_whole = lax.all_gather(down_weight, "sp", axis=1, tiled=True)
    hidden = (jax.nn.silu(gate_sums) * up_sums).astype(jnp.bfloat16)
    channel_out = lax.psum_scatter(
        jnp.dot(hidden, down_whole, preferred_element_type=jnp.float32).astype(jnp.bfloat16),
        "tp",
        scatter_dimension=0,
        tiled=True,
    ).astype(jnp.float32)
    return (middle.astype(jnp.float32) + channel_out).astype(jnp.bfloat16)


MESH = pl.DeviceIdType.MESH
LANES = 128
PAIR = 2


def kernel(
    n_sp,
    query_hbm,
    latent_hbm,
    latent_gain_ref,
    key_weight_hbm,
    value_weight_hbm,
    output_gain_ref,
    mixer_gain_ref,
    cos_hbm,
    sin_hbm,
    residual_hbm,
    output_weight_hbm,
    turn_hbm,
    rotary_hbm,
    gate_ref,
    up_ref,
    down_ref,
    out_ref,
    query_ref,
    latent_ref,
    key_weight_ref,
    value_weight_ref,
    cos_ref,
    sin_ref,
    residual_ref,
    output_weight_ref,
    turn_ref,
    rotary_ref,
    lat_all,
    rot_all,
    rot_keys,
    keys,
    values,
    projected,
    to_core_rows,
    from_core_rows,
    to_x_rows,
    from_x_rows,
    middle,
    normed,
    gate_all,
    up_all,
    down_all,
    gates,
    hidden,
    part,
    from_core,
    to_x,
    from_x,
    to_z,
    from_z,
    summed_up,
    send_sems,
    recv_sems,
    local_sems,
):
    n_z = n_sp // PAIR
    s = lax.axis_index("sp")
    t = lax.axis_index("tp")
    z, y = s // PAIR, lax.rem(s, PAIR)
    x, c = t // PAIR, lax.rem(t, PAIR)
    rows, depth = latent_ref.shape
    half = rows // PAIR
    sibling = (s, x * PAIR + 1 - c)
    across = (s, (1 - x) * PAIR + c)
    beside = (z * PAIR + 1 - y, t)
    f32 = jnp.float32
    bf16 = jnp.bfloat16

    def other(step):
        if step == 0:
            return z
        if step == 1:
            return z + 1 - 2 * lax.rem(z, PAIR)
        if step == 2:
            return lax.rem(z + PAIR, n_z)
        return n_z - 1 - z

    def z_id(step):
        return (other(step) * PAIR + y, t)

    barrier = pltpu.get_barrier_semaphore()
    greeted = [z_id(k) for k in range(1, n_z)] + [beside, sibling, across]
    for device in greeted:
        pl.semaphore_signal(barrier, inc=1, device_id=device, device_id_type=MESH)

    used = [0]
    locals_used = [0]
    sent = []

    def local(src, dst, go=None):
        copy = pltpu.make_async_copy(src, dst, local_sems.at[locals_used[0]])
        locals_used[0] += 1
        if go is None:
            copy.start()
        else:
            pl.when(go)(copy.start)
        return (copy, go)

    def landed(pair):
        copy, go = pair
        if go is None:
            copy.wait()
        else:
            pl.when(go)(copy.wait)

    def send(src, dst, device, go=None, comes=None):
        copy = pltpu.make_async_remote_copy(
            src_ref=src,
            dst_ref=dst,
            send_sem=send_sems.at[used[0]],
            recv_sem=recv_sems.at[used[0]],
            device_id=device,
            device_id_type=MESH,
        )
        used[0] += 1
        if go is None:
            copy.start()
        else:
            pl.when(go)(copy.start)
        sent.append((copy, go))
        return (copy, comes)

    def arrived(*pairs):
        for copy, comes in pairs:
            if comes is None:
                copy.wait_recv()
            else:
                pl.when(comes)(copy.wait_recv)

    locals_first = [
        local(latent_hbm, latent_ref),
        local(rotary_hbm, rotary_ref),
        local(turn_hbm, turn_ref),
        local(query_hbm, query_ref),
        local(key_weight_hbm, key_weight_ref),
        local(value_weight_hbm, value_weight_ref),
        local(cos_hbm, cos_ref),
        local(sin_hbm, sin_ref),
    ]
    locals_rest = [
        local(output_weight_hbm, output_weight_ref),
        local(residual_hbm, residual_ref),
    ]

    width = gate_all.shape[1]
    total_width = gate_ref.shape[1]
    slab = gate_ref.shape[0]
    main = width - LANES
    short = n_z * width - total_width

    def full(owner):
        return jnp.where(c == 0, owner, n_z - 1 - owner) > 0

    def first(owner):
        return pl.multiple_of(jnp.maximum(owner * width - (1 - c) * short, 0), LANES)

    def span(owner):
        return pl.ds(pl.multiple_of(owner * slab, slab), slab)

    mine = span(s)
    mine_full = full(z)
    low, high = pl.ds(0, main), pl.ds(main, LANES)
    down_cols = pl.ds(pl.multiple_of(y * slab, slab), slab)

    def unit_parts(owner):
        start = first(owner)
        last = jnp.minimum(start + main, total_width - LANES)
        return pl.ds(start, main), pl.ds(pl.multiple_of(last, LANES), LANES)

    def wide_ends(ref, buffer, owner):
        a, b = unit_parts(owner)
        return [
            (ref.at[:, a], buffer.at[mine, low]),
            (ref.at[:, b], buffer.at[mine, high]),
        ]

    def down_ends(owner, step):
        a, b = unit_parts(owner)
        return [
            (down_ref.at[a], down_all.at[step, low, down_cols]),
            (down_ref.at[b], down_all.at[step, high, down_cols]),
        ]

    def send_parts(ends, device, go):
        return [
            send(*ends[0], device),
            send(*ends[1], device, go=go, comes=mine_full),
        ]

    def local_parts(ends):
        return [local(*ends[0]), local(*ends[1], go=mine_full)]

    def gate_to(k):
        return send_parts(wide_ends(gate_ref, gate_all, other(k)), z_id(k), full(other(k)))

    def up_to(k):
        return send_parts(wide_ends(up_ref, up_all, other(k)), z_id(k), full(other(k)))

    def down_to(k):
        return send_parts(down_ends(other(k), k), z_id(k), full(other(k)))

    def relay_wide(copies, buffer, step):
        arrived(*copies)
        block = span(other(step) * PAIR + y)
        ends = [(buffer.at[block, cols],) * 2 for cols in (low, high)]
        return send_parts(ends, beside, mine_full)

    def relay_down(copies, step):
        arrived(*copies)
        ends = [(down_all.at[step, units, down_cols],) * 2 for units in (low, high)]
        return send_parts(ends, beside, mine_full)

    weights_here = (
        local_parts(wide_ends(gate_ref, gate_all, z))
        + local_parts(wide_ends(up_ref, up_all, z))
        + local_parts(down_ends(z, 0))
    )

    @pl.when(jnp.logical_not(mine_full))
    def _():
        down_all[:, main:, :] = jnp.zeros((n_z, LANES, down_all.shape[2]), bf16)

    for copy in locals_first[:2]:
        landed(copy)
    pl.semaphore_wait(barrier, len(greeted))

    half_rows = pl.ds(pl.multiple_of(c * half, half), half)
    rot_half = rotary_ref.shape[0] // PAIR
    rot_rows = pl.ds(pl.multiple_of(c * rot_half, rot_half), rot_half)

    def token_half(owner):
        return pl.ds(pl.multiple_of(owner * rows + c * half, half), half)

    def send_latent(device):
        return [
            send(latent_ref.at[half_rows], lat_all.at[token_half(s)], device),
            send(rotary_ref.at[rot_rows], rot_all.at[s, rot_rows], device),
        ]

    def pass_latent(owner, device):
        place = token_half(owner)
        return [
            send(lat_all.at[place], lat_all.at[place], device),
            send(rot_all.at[owner, rot_rows], rot_all.at[owner, rot_rows], device),
        ]

    steps = list(range(1, n_z))
    far_first = [2, 3, 1]
    latent_z = {k: send_latent(z_id(k)) for k in far_first}
    latent_y = {0: send_latent(beside)}
    gate_z = {k: gate_to(k) for k in far_first}
    up_z = {2: up_to(2)}
    gate_y = [
        send_parts(wide_ends(gate_ref, gate_all, z), beside, mine_full),
    ]

    latent_core = []
    for k in (1, 2, 3):
        arrived(*latent_z[k])
        owner = other(k) * PAIR + y
        latent_y[k] = pass_latent(owner, beside)
        latent_core += pass_latent(owner, sibling)
    up_y = [send_parts(wide_ends(up_ref, up_all, z), beside, mine_full)]
    down_y = {0: send_parts(down_ends(z, 0), beside, mine_full)}
    for k in (0, 1, 2, 3):
        arrived(*latent_y[k])
        latent_core += pass_latent(other(k) * PAIR + 1 - y, sibling)
    for copy in locals_first[2:]:
        landed(copy)

    gain = latent_gain_ref[...]
    here = pl.ds(pl.multiple_of(s * rows, rows), rows)
    lat_all[here, :] = latent_ref[...]
    rot_all[s] = rotary_ref[...]
    arrived(*latent_core)

    def project(block, _):
        place = pl.ds(pl.multiple_of(block * rows, rows), rows)
        raw = lat_all[place, :].astype(f32)
        scale = lax.rsqrt(jnp.mean(raw * raw, axis=-1, keepdims=True) + epsilon)
        latent = (raw * scale * gain).astype(bf16)
        keys[place, :] = jnp.dot(latent, key_weight_ref[...], preferred_element_type=f32).astype(
            bf16
        )
        values[place, :] = jnp.dot(
            latent, value_weight_ref[...], preferred_element_type=f32
        ).astype(bf16)
        return 0

    lax.fori_loop(0, n_sp, project, 0)

    def turn(raw, cosine, sine):
        top, bottom = raw[:rot_half].astype(f32), raw[rot_half:].astype(f32)
        return jnp.concatenate(
            [top * cosine - bottom * sine, bottom * cosine + top * sine], axis=0
        )

    for block in range(n_sp):
        cols = slice(block * rows, (block + 1) * rows)
        rot_keys[:, cols] = turn(rot_all[block], cos_ref[block], sin_ref[block]).astype(bf16)

    content = query_ref.shape[1]
    rot_width = rotary_ref.shape[0]
    head_count = turn_ref.shape[0] // rot_width
    my_cos, my_sin = cos_ref[s], sin_ref[s]
    turned = [
        turn(turn_ref[index * rot_width : (index + 1) * rot_width], my_cos, my_sin)
        for index in range(head_count)
    ]
    turned.append(jnp.zeros((LANES - head_count * rot_width, rows), f32))
    turned = jnp.transpose(jnp.concatenate(turned, axis=0)).astype(bf16)

    wide_dev = (content - head_count * NARROW_DIM) // (WIDE_DIM - NARROW_DIM)
    sizes = [NARROW_DIM] * (head_count - wide_dev) + [WIDE_DIM] * wide_dev
    contract = (((1,), (1,)), ((), ()))
    heads = []
    start = 0
    for index, size in enumerate(sizes):
        cols = slice(start, start + size)
        scores = lax.dot_general(
            query_ref[:, cols], keys[:, cols], contract, preferred_element_type=f32
        )
        scores = scores + jnp.dot(
            turned[:, index * rot_width : (index + 1) * rot_width],
            rot_keys[...],
            preferred_element_type=f32,
        )
        scores = scores * (size + ROT_DIM) ** (-0.5)
        powers = jnp.exp(scores - jnp.max(scores, axis=-1, keepdims=True))
        totals = jnp.sum(powers, axis=-1, keepdims=True)
        summed = jnp.dot(powers.astype(bf16), values[:, cols], preferred_element_type=f32)
        attended = summed / totals
        scale = lax.rsqrt(jnp.mean(attended * attended, axis=-1, keepdims=True) + epsilon)
        heads.append(attended * scale)
        start += size
    mixed = (jnp.concatenate(heads, axis=1) * output_gain_ref[...]).astype(bf16)

    for copy in locals_rest:
        landed(copy)
    projected[...] = jnp.dot(
        mixed, output_weight_ref[...], preferred_element_type=f32
    ).reshape(projected.shape)
    to_core_rows[...] = projected[:, 1 - c].astype(bf16)
    rows_core = send(to_core_rows, from_core_rows, sibling)
    gate_y.append(relay_wide(gate_z[1], gate_all, 1))
    arrived(rows_core)
    to_x_rows[...] = (projected[1 - x, c] + from_core_rows[1 - x].astype(f32)).astype(bf16)
    rows_x = send(to_x_rows, from_x_rows, across)
    near_rows = projected[x, c] + from_core_rows[x].astype(f32) + residual_ref[...].astype(f32)
    gate_y.append(relay_wide(gate_z[2], gate_all, 2))
    arrived(rows_x)
    middle[...] = (near_rows + from_x_rows[...].astype(f32)).astype(bf16)
    tall = middle[...].astype(f32)
    scale = lax.rsqrt(jnp.mean(tall * tall, axis=-1, keepdims=True) + epsilon)
    normed[z, t] = (tall * scale * mixer_gain_ref[...]).astype(bf16)

    def pass_normed(owner, place, device):
        return send(normed.at[owner, place], normed.at[owner, place], device)

    normed_z = {k: pass_normed(z, t, z_id(k)) for k in far_first}
    normed_x = {0: pass_normed(z, t, across)}
    normed_core = [pass_normed(z, t, sibling)]
    for k in (3, 1):
        up_z[k] = up_to(k)
    down_z = {k: down_to(k) for k in (1, 2, 3)}
    gate_y.append(relay_wide(gate_z[3], gate_all, 3))
    up_y.append(relay_wide(up_z[2], up_all, 2))

    for k in (1, 2, 3):
        arrived(normed_z[k])
        normed_x[k] = pass_normed(other(k), t, across)
        normed_core.append(pass_normed(other(k), t, sibling))
    far_t = (1 - x) * PAIR + c
    for k in range(n_z):
        arrived(normed_x[k])
        normed_core.append(pass_normed(other(k), far_t, sibling))
    for copy in weights_here:
        landed(copy)
    for copies in gate_y:
        arrived(*copies)
    arrived(*normed_core)

    d_model = middle.shape[1]

    def gate_units(block, _):
        place = pl.ds(pl.multiple_of(block * rows, rows), rows)
        left = normed[block].reshape(rows, d_model)
        gates[place, :] = jnp.dot(left, gate_all[...], preferred_element_type=f32)
        return 0

    lax.fori_loop(0, n_z, gate_units, 0)

    for k in (3, 1):
        up_y.append(relay_wide(up_z[k], up_all, k))
    for copies in up_y:
        arrived(*copies)

    lane = lax.broadcasted_iota(jnp.int32, (rows, width), 1)
    fresh = lane < jnp.where(mine_full, width, main)

    def units(block, _):
        place = pl.ds(pl.multiple_of(block * rows, rows), rows)
        left = normed[block].reshape(rows, d_model)
        ups = jnp.dot(left, up_all[...], preferred_element_type=f32)
        gate = gates[place, :]
        value = gate / (1.0 + jnp.exp(-gate)) * ups
        hidden[place, :] = jnp.where(fresh, value, 0.0).astype(bf16)
        return 0

    lax.fori_loop(0, n_z, units, 0)

    down_y[1] = relay_down(down_z[1], 1)
    core_copies, x_copies, z_copies = [], [], []
    for step in range(n_z + 2):
        n = step - 2
        if 0 <= n < n_z:
            arrived(x_copies[n])
            to_z[n] = (to_x[n, :, x].astype(f32) + from_x[n].astype(f32)).astype(bf16)
            z_copies.append(
                {
                    k: send(to_z.at[n, other(k)], from_z.at[n, k - 1], z_id(k))
                    for k in far_first
                }
            )
        n = step - 1
        if 0 <= n < n_z:
            arrived(core_copies[n])
            to_x[n] = (part[n, :, :, c].astype(f32) + from_core[n].astype(f32)).astype(bf16)
            x_copies.append(send(to_x.at[n, :, 1 - x], from_x.at[n], across))
        n = step
        if n < n_z:
            if 2 <= n + 1 < n_z:
                down_y[n + 1] = relay_down(down_z[n + 1], n + 1)
            arrived(*down_y[n])
            product = jnp.dot(hidden[...], down_all[n], preferred_element_type=f32)
            part[n] = product.astype(bf16).reshape(part.shape[1:])
            core_copies.append(send(part.at[n, :, :, 1 - c], from_core.at[n], sibling))
    chunk = part.shape[-1]

    def cols_of(step):
        return pl.ds(pl.multiple_of(other(step) * chunk, chunk), chunk)

    for n in range(n_z):
        cols = cols_of(n)
        summed_up[:, cols] = middle[:, cols].astype(f32) + to_z[n, z].astype(f32)
    for n in range(n_z):
        for k in steps:
            arrived(z_copies[n][k])
            cols = cols_of(n ^ k)
            summed_up[:, cols] = summed_up[:, cols] + from_z[n, k - 1].astype(f32)
    out_ref[...] = summed_up[...].astype(bf16)
    for copy, go in sent:
        if go is None:
            copy.wait_send()
        else:
            pl.when(go)(copy.wait_send)


def fused(
    n_sp,
    residual,
    query_content,
    query_rotary,
    key_latent,
    rotary_key,
    latent_gain,
    key_weight,
    value_weight,
    output_gain,
    output_weight,
    mixer_gain,
    gate_weight,
    up_weight,
    down_weight,
):
    n_z = n_sp // PAIR
    rows, latent_width = key_latent.shape
    strip, d_model = residual.shape
    tokens = rows * n_sp
    content = query_content.shape[1]
    turn_width = query_rotary.shape[1]
    half_width = ROT_DIM // 2
    inverse = np.float32(1.0) / np.power(
        np.float32(rope_base), np.arange(0, ROT_DIM, 2, dtype=np.float32) / np.float32(ROT_DIM)
    )
    angles = np.arange(tokens, dtype=np.float32)[:, None] * inverse[None, :].astype(np.float32)
    angles = angles.reshape(n_sp, rows, half_width).transpose(0, 2, 1)
    cos_table = np.cos(angles).astype(np.float32)
    sin_table = np.sin(angles).astype(np.float32)
    tiles = gate_weight.shape[1] // LANES
    width = -(-tiles // n_z) * LANES
    slab = rows * n_z
    chunk = d_model // n_z
    bf16 = jnp.bfloat16
    n_copies = 16 * n_sp
    vmem = pl.BlockSpec(memory_space=pltpu.VMEM)
    anywhere = pl.BlockSpec(memory_space=pl.ANY)
    return pl.pallas_call(
        functools.partial(kernel, n_sp),
        out_shape=jax.ShapeDtypeStruct((strip, d_model), bf16),
        in_specs=[anywhere] * 2 + [vmem] + [anywhere] * 2 + [vmem] * 2 + [anywhere] * 9,
        out_specs=vmem,
        scratch_shapes=[
            pltpu.VMEM((rows, content), bf16),
            pltpu.VMEM((rows, latent_width), bf16),
            pltpu.VMEM((latent_width, content), bf16),
            pltpu.VMEM((latent_width, content), bf16),
            pltpu.VMEM((n_sp, half_width, rows), jnp.float32),
            pltpu.VMEM((n_sp, half_width, rows), jnp.float32),
            pltpu.VMEM((strip, d_model), bf16),
            pltpu.VMEM((content, d_model), bf16),
            pltpu.VMEM((turn_width, rows), bf16),
            pltpu.VMEM((ROT_DIM, rows), bf16),
            pltpu.VMEM((tokens, latent_width), bf16),
            pltpu.VMEM((n_sp, ROT_DIM, rows), bf16),
            pltpu.VMEM((ROT_DIM, tokens), bf16),
            pltpu.VMEM((tokens, content), bf16),
            pltpu.VMEM((tokens, content), bf16),
            pltpu.VMEM((PAIR, PAIR, strip, d_model), jnp.float32),
            pltpu.VMEM((PAIR, strip, d_model), bf16),
            pltpu.VMEM((PAIR, strip, d_model), bf16),
            pltpu.VMEM((strip, d_model), bf16),
            pltpu.VMEM((strip, d_model), bf16),
            pltpu.VMEM((strip, d_model), bf16),
            pltpu.VMEM((n_z, PAIR * PAIR, strip, d_model), bf16),
            pltpu.VMEM((d_model, width), bf16),
            pltpu.VMEM((d_model, width), bf16),
            pltpu.VMEM((n_z, width, chunk), bf16),
            pltpu.VMEM((slab, width), jnp.float32),
            pltpu.VMEM((slab, width), bf16),
            pltpu.VMEM((n_z, n_z, PAIR, PAIR, strip, chunk), bf16),
            pltpu.VMEM((n_z, n_z, PAIR, strip, chunk), bf16),
            pltpu.VMEM((n_z, n_z, PAIR, strip, chunk), bf16),
            pltpu.VMEM((n_z, n_z, strip, chunk), bf16),
            pltpu.VMEM((n_z, n_z, strip, chunk), bf16),
            pltpu.VMEM((n_z, n_z - 1, strip, chunk), bf16),
            pltpu.VMEM((strip, d_model), jnp.float32),
            pltpu.SemaphoreType.DMA((n_copies,)),
            pltpu.SemaphoreType.DMA((n_copies,)),
            pltpu.SemaphoreType.DMA((2 * n_sp,)),
        ],
        compiler_params=pltpu.CompilerParams(
            collective_id=0, has_side_effects=True, vmem_limit_bytes=60 * 1024 * 1024
        ),
        name="layer",
    )(
        query_content,
        key_latent,
        latent_gain.reshape(1, -1),
        key_weight,
        value_weight,
        output_gain.reshape(1, -1),
        mixer_gain.reshape(1, -1),
        jnp.asarray(cos_table),
        jnp.asarray(sin_table),
        residual,
        output_weight,
        query_rotary.T,
        rotary_key.T,
        gate_weight,
        up_weight,
        down_weight,
    )


def solution(mesh):
    n_sp, n_tp = mesh.shape["sp"], mesh.shape["tp"]

    def program(*arrays):
        residual, gate_weight = arrays[0], arrays[11]
        fits = (
            n_tp == PAIR * PAIR
            and n_sp == PAIR**3
            and gate_weight.shape[0] * n_sp == residual.shape[1]
            and gate_weight.shape[0] % LANES == 0
            and gate_weight.shape[1] % LANES == 0
            and -(gate_weight.shape[1] // LANES) % (n_sp // PAIR) == 1
            and arrays[3].shape[0] == LANES
        )
        if fits:
            return fused(n_sp, *arrays)
        return on_device(*arrays)

    placed = (
        P(("sp", "tp"), None),
        P("sp", "tp"),
        P("sp", "tp"),
        P("sp", None),
        P("sp", None),
        P(),
        P(None, "tp"),
        P(None, "tp"),
        P("tp"),
        P("tp", None),
        P(),
        P("sp", "tp"),
        P("sp", "tp"),
        P("tp", "sp"),
    )
    return jax.shard_map(
        program, mesh=mesh, in_specs=placed, out_specs=P(("sp", "tp"), None), check_vma=False
    )
```

time: 112 us -> 101 us (0.902)
  Pallas kernels: 108 us -> 99.3 us
  local copies, waits for them, and re-layouts: 3.75 us -> 1.57 us
    pallas_call x1, Pallas kernels: 108 us -> 99.3 us  [fused(): pl.pallas_call(functools.partial(kernel, n_sp), out_shape=jax.ShapeDtypeS...]
    unnamed x5 -> x1, local copies, waits for them, and re-layouts: 3.75 us -> 1.57 us
where the time goes in v1:
time: 101 us
  Pallas kernels  99.3 us (98%)
  local copies, waits for them, and re-layouts  1.57 us (2%)
    pallas_call x1, Pallas kernels, fused(): pl.pallas_call(functools.partial(kernel, n_sp), out_shape=jax.ShapeDtypeS...  99.3 us

profile of v1, /device:TPU:0, one launch (start us, length us, event | category | flops | bytes accessed | tf_op | source)
XLA Modules:
  0.0 100.9 jit_solution(3861250765108008155)
XLA Ops:
  0.0 99.3 %layer.1 = bf16[32,2048]{1,0:T(8,128)(2,1)} custom-call(bf16[128,256]{1,0:T(8,128)(2,1)} %query_hbm.1, bf16[128,512]{1,0:T(8,128)(2,1)} %latent_hbm.1, f32[1,512]{1,0:T(1,128)} %bitcast.8, bf16[512,256]{1,0:T(8,128)(2,1)} %key_weight_hbm.1, bf16[512,256]{1,0:T(8,128)(2,1)} %value_weight_hbm.1, f32[1,256]{1,0:T(1,128)} %bitcast.9, f32[1,2048]{1,0:T(1,128)} %bitcast.6, ...), custom_call_target="tpu_custom_call" | custom-call | tf_op jit(solution)/shard_map/layer/pallas_call | solution.py:670
  99.4 1.6 %copy.18 = bf16[32,2048]{1,0:T(8,128)(2,1)} copy(bf16[32,2048]{1,0:T(8,128)(2,1)} %layer.1) | data formatting | bytes 262144
